TPU v7x, 512 devices: a whole 4x8x8 slice. The times are simulated.
512 devices in a mesh: sp: 64 (over z, y), tp: 8 (over x, core).
Axes of the slice: x: 4, y: 8, z: 8, core: 2. Of those that a mesh axis runs over, the one named last changes fastest.
Arguments:
- tokens_in: bfloat16 [16384, 2048], P('sp', 'tp'), may hold values from -400 to 400
- norm_gain: float32 [2048], replicated, may hold values from 0.1 to 1.9
- w_query: bfloat16 [2048, 1024], P('sp', 'tp'), may hold values from -0.125 to 0.125
- w_forget: bfloat16 [2048, 1024], P('sp', 'tp'), may hold values from -0.125 to 0.125
- w_input: bfloat16 [2048, 1024], P('sp', 'tp'), may hold values from -0.125 to 0.125
- w_rgate: bfloat16 [2048, 1024], P('sp', 'tp'), may hold values from -0.125 to 0.125
- w_pool_in: bfloat16 [2048, 1024], P('sp', 'tp'), may hold values from -0.125 to 0.125
- w_pgate: bfloat16 [2048, 1024], P('sp', 'tp'), may hold values from -0.125 to 0.125
- floor_rate: float32 [1024], P('tp'), as said below
- extra_logdecay: float32 [16384, 8], P('sp', 'tp'), as said below
- state_gain: float32 [1024], P('tp'), may hold values from 0.1 to 1.9
- pool_mix: bfloat16 [8, 128, 128], P('tp'), may hold values from -0.5 to 0.5
- pool_gain: float32 [1024], P('tp'), may hold values from 0.1 to 1.9
- out_rec: bfloat16 [1024, 2048], P('tp', 'sp'), may hold values from -0.125 to 0.125
- out_pool: bfloat16 [1024, 2048], P('tp', 'sp'), may hold values from -0.125 to 0.125
- post_gain: float32 [2048], replicated, may hold values from 0.1 to 1.9
Outputs:
- mixed_out: bfloat16 [16384, 2048], P(('sp', 'tp'))
Inputs may be any that keep to these rules, and one draw needn't show every extreme that they name: `floor_rate`: every entry is positive. `extra_logdecay`: every entry is at most zero.
All inputs are finite; a program needn't handle non-finite values.
Results may differ from a plain program's by a relative error of at most 0.015.
Values may be sent and summed in bfloat16 or wider, within the bound.
A program may use at most 64 MiB of HBM per device.

v0:
```python
import jax
import jax.numpy as jnp
from jax import lax
from jax.sharding import Mesh
from jax.sharding import PartitionSpec as P

DK = 128
BLOCK = 64
SP = ("sp_0", "sp_1")
TP = ("tp_0", "tp_1")
SP_TP = ("sp_0", "sp_1", "tp_0", "tp_1")
eps = 1e-06
coarsest_scale_depth = lax.Precision.HIGHEST


def in_one_piece(arrays, axis, dim, along):
    widths = [a.shape[along] for a in arrays]
    both = jnp.concatenate(arrays, axis=along)
    out = lax.all_gather(both, axis, axis=dim, tiled=True)
    return tuple(jnp.split(out, [sum(widths[:k]) for k in range(1, len(widths))], axis=along))


def cut_rows(length, count):
    turn = length // count
    if turn >= 8:
        turn -= turn % 8
    return [turn * k for k in range(1, count)]


def all_blocks(shard, axes, order):
    tiles = shard[None]
    for k in order:
        tiles = lax.all_gather(tiles, axes[k], axis=0, tiled=True)
    held = [lax.axis_size(axes[k]) for k in reversed(order)]
    tiles = tiles.reshape(*held, *shard.shape)
    turned = sorted(range(len(order)), key=lambda place: order[len(order) - 1 - place])
    return tiles.transpose(*turned, *range(len(order), tiles.ndim)).reshape(-1, *shard.shape)


def joined_along(tiles, dim):
    tiles = jnp.moveaxis(tiles, 0, dim)
    lengths = tiles.shape
    return tiles.reshape(*lengths[:dim], lengths[dim] * lengths[dim + 1], *lengths[dim + 2 :])


def gather_at_once(shard, axes, dim):
    widest = max(range(max(1, shard.ndim - 1)), key=lambda d: shard.shape[d])
    count, done = (len(axes), [])
    for initial, piece in enumerate(
        jnp.split(shard, cut_rows(shard.shape[widest], count), axis=widest)
    ):
        if piece.size:
            order = [(initial - k) % count for k in range(count)]
            done.append(all_blocks(piece, axes, order))
    return joined_along(jnp.concatenate(done, axis=widest + 1), dim)


def nothing_yet(shard, identity):
    return jax.tree.map(
        lambda part, zero: jnp.zeros_like(part) + jnp.asarray(zero, part.dtype), shard, identity
    )


def all_in_one(shard, axis):
    leaves = jax.tree.leaves(shard)
    order = sorted(range(len(leaves)), key=lambda k: -leaves[k].size)
    width = (1, *leaves[order[0]].shape)[-1]
    lines = [
        jnp.pad(leaves[k].reshape(-1), (0, -leaves[k].size % width)).reshape(-1, width)
        for k in order
    ]
    both, at, found = (lax.all_gather(jnp.concatenate(lines), axis), 0, {})
    for k, line in zip(order, lines):
        piece = both[:, at : at + len(line)].reshape(len(both), -1)
        found[k] = piece[:, : leaves[k].size].reshape(-1, *leaves[k].shape)
        at += len(line)
    numbers = iter(range(len(leaves)))
    return jax.tree.map(lambda _: found[next(numbers)], shard)


def prefix_by_axis(shard, axes, combine, identity):
    before = start = nothing_yet(shard, identity)
    so_far = shard
    for axis in reversed(axes):
        peers, index = (lax.axis_size(axis), lax.axis_index(axis))
        pieces = all_in_one(so_far, axis)
        inside, so_far = (start, start)
        for k in range(peers):
            passed = k < index
            so_far = combine(so_far, jax.tree.map(lambda part: part[k], pieces))
            inside = jax.tree.map(lambda new, old: jnp.where(passed, new, old), so_far, inside)
        before = combine(inside, before)
    return before


def shifted(value, axis, steps):
    count = lax.axis_size(axis)
    initial, last = (max(0, -steps), min(count, count - steps))
    return lax.ppermute(value, axis, [(source, source + steps) for source in range(initial, last)])


def gather_turned(arrays, axis, dims):
    turned = [jnp.moveaxis(a, dim, 0) for a, dim in zip(arrays, dims)]
    widths = [t[0].size for t in turned]
    both = jnp.concatenate([t.reshape(-1, w) for t, w in zip(turned, widths)], axis=1)
    out = lax.all_gather(both, axis, axis=0, tiled=True)
    tiles = jnp.split(out, [sum(widths[:k]) for k in range(1, len(widths))], axis=1)
    return tuple(
        (
            jnp.moveaxis(b.reshape(-1, *t.shape[1:]), 0, dim)
            for b, t, dim in zip(tiles, turned, dims)
        )
    )


def chain_merge(earlier, later):
    return (earlier[0] * later[0], later[0][..., None] * earlier[1] + later[1])


def local_blocks(qs, keys, values, logs):
    causal = jnp.arange(BLOCK)[:, None] >= jnp.arange(BLOCK)[None, :]
    heads_dev = qs.shape[1]

    def advance(carry, member):
        carried_memory_matrix, start = carry
        probe_segment, key_piece, input_piece, gc = member
        prefix_sum_vector = jnp.cumsum(gc, axis=1)
        last_index = prefix_sum_vector[:, -1]
        cross_segment_contribution = jnp.einsum(
            "abz,azy->aby",
            probe_segment * jnp.exp(prefix_sum_vector),
            carried_memory_matrix,
            precision=coarsest_scale_depth,
        )
        diff = prefix_sum_vector[:, :, None, :] - prefix_sum_vector[:, None, :, :]
        weight = jnp.where(causal[None, :, :, None], jnp.exp(jnp.minimum(diff, 0.0)), 0.0)
        scores = jnp.einsum(
            "htk,hsk,htsk->hts", probe_segment, key_piece, weight, precision=coarsest_scale_depth
        )
        final_result = cross_segment_contribution + jnp.einsum(
            "hts,hsv->htv", scores, input_piece, precision=coarsest_scale_depth
        )
        carried_memory_matrix = jnp.exp(last_index)[..., None] * carried_memory_matrix + jnp.einsum(
            "njp,njq->npq",
            key_piece * jnp.exp(last_index[:, None, :] - prefix_sum_vector),
            input_piece,
            precision=coarsest_scale_depth,
        )
        pool_reach = probe_segment * jnp.exp(start[:, None, :] + prefix_sum_vector)
        return ((carried_memory_matrix, start + last_index), (final_result, pool_reach))

    begin = (jnp.zeros((heads_dev, DK, DK), jnp.float32), jnp.zeros((heads_dev, DK), jnp.float32))
    (carried_memory_matrix, total), (final_result, pool_reach) = lax.scan(
        advance, begin, (qs, keys, values, logs)
    )
    return (carried_memory_matrix, total, final_result, pool_reach)


def per_device(
    tokens_in,
    norm_gain,
    w_query,
    w_forget,
    w_input,
    w_rgate,
    w_pool_in,
    w_pgate,
    floor_rate,
    extra_logdecay,
    state_gain,
    pool_mix,
    pool_gain,
    out_rec,
    out_pool,
    post_gain,
):
    gathered = in_one_piece((w_query, w_forget, w_input, w_rgate, w_pool_in, w_pgate), SP, 0, 1)
    joined = jnp.concatenate(gathered, axis=1)
    head_cols = w_query.shape[1]
    positions = tokens_in.shape[0]
    model_width = norm_gain.shape[0]
    wide = gather_at_once(tokens_in, TP, 1).astype(jnp.float32)
    scaled = (wide * norm_gain[None, :]).astype(jnp.bfloat16)
    totals = jnp.dot(scaled, joined, preferred_element_type=jnp.float32)
    squares = jnp.sum(wide * wide, axis=1)
    inv_rms = lax.rsqrt(squares / model_width + eps)
    proj = (totals * inv_rms[:, None]).astype(jnp.bfloat16)
    query = proj[:, 0:head_cols]
    forget = proj[:, head_cols : 2 * head_cols]
    inputs = proj[:, 2 * head_cols : 3 * head_cols]
    rgate = proj[:, 3 * head_cols : 4 * head_cols]
    pool_in = proj[:, 4 * head_cols : 5 * head_cols]
    pgate = proj[:, 5 * head_cols : 6 * head_cols]
    heads_dev = head_cols // DK
    blocks = positions // BLOCK

    def to_blocks(array):
        return array.reshape(blocks, BLOCK, heads_dev, DK).transpose(0, 2, 1, 3)

    forget32 = forget.astype(jnp.float32)
    key_gate = -jnp.expm1(-floor_rate)[None, :] * jax.nn.sigmoid(-forget32)
    log_forget = jnp.log1p(-key_gate) + jnp.repeat(extra_logdecay, DK, axis=1)
    qs = query.astype(jnp.float32) * DK ** (-0.5)
    carried_memory_matrix, total, final_result, pool_reach = local_blocks(
        to_blocks(qs),
        to_blocks(key_gate),
        to_blocks(inputs.astype(jnp.float32)),
        to_blocks(log_forget),
    )
    decays = jnp.exp(total)
    tail_rows = pool_in[positions - 16 :]
    carried = prefix_by_axis(
        (decays, carried_memory_matrix),
        SP,
        chain_merge,
        (jnp.ones_like(decays), jnp.zeros_like(carried_memory_matrix)),
    )
    incoming_state = carried[1]
    previous = shifted(tail_rows, SP, 1).astype(jnp.float32)
    recurrent_output = final_result + jnp.einsum(
        "izaf,zfu->izau", pool_reach, incoming_state, precision=coarsest_scale_depth
    )
    grouped = recurrent_output.transpose(0, 2, 1, 3).reshape(positions, heads_dev, DK)
    normed = grouped * lax.rsqrt(jnp.mean(grouped * grouped, axis=2, keepdims=True) + eps)
    y_rec = (
        normed.reshape(positions, head_cols)
        * state_gain[None, :]
        * jax.nn.silu(rgate.astype(jnp.float32))
    ).astype(jnp.bfloat16)
    group = lax.axis_index(TP) * heads_dev + jnp.arange(head_cols) // DK
    window = jnp.power(2, 1 + group % 4).astype(jnp.int32)
    pool32 = pool_in.astype(jnp.float32)
    extended = jnp.concatenate([previous, pool32], axis=0)
    summed_rows = jnp.zeros((positions, head_cols), jnp.float32)
    for offset in range(16):
        rows_back = extended[16 - offset : 16 - offset + positions]
        summed_rows = summed_rows + jnp.where((offset < window)[None, :], rows_back, 0.0)
    place = lax.axis_index(SP) * positions + jnp.arange(positions)
    count = jnp.minimum(place[:, None] + 1, window[None, :]).astype(jnp.float32)
    mixed = (summed_rows / count - pool32).astype(jnp.bfloat16)
    mapped = jnp.einsum(
        "tgc,gcd->tgd",
        mixed.reshape(positions, heads_dev, DK),
        pool_mix,
        preferred_element_type=jnp.float32,
    ).reshape(positions, head_cols)
    y_pool = (mapped * pool_gain[None, :] * jax.nn.silu(pgate.astype(jnp.float32))).astype(
        jnp.bfloat16
    )
    out_parts = gather_turned((out_rec, out_pool), SP, (1, 1))
    both = jnp.concatenate([y_rec, y_pool], axis=1)
    weight_cat = jnp.concatenate(out_parts, axis=0)
    groups = lax.axis_size(TP)
    exchanged = lax.all_to_all(both, TP, split_axis=0, concat_axis=1, tiled=True)
    whole = lax.all_gather(weight_cat, TP, axis=0, tiled=True)
    owned = exchanged.shape[0]
    terms = jnp.einsum(
        "tjc,jcd->jtd",
        exchanged.reshape(owned, groups, 2 * head_cols),
        whole.reshape(groups, 2 * head_cols, model_width),
        preferred_element_type=jnp.float32,
    )
    summed = jnp.sum(terms.astype(jnp.bfloat16).astype(jnp.float32), axis=0)
    final = (
        summed
        * lax.rsqrt(jnp.mean(summed * summed, axis=1, keepdims=True) + eps)
        * post_gain[None, :]
    )
    return final.astype(jnp.bfloat16)


def solution(mesh):
    torus = Mesh(mesh.devices.reshape(8, 8, 4, 2), ("sp_0", "sp_1", "tp_0", "tp_1"))
    return jax.shard_map(
        per_device,
        mesh=torus,
        in_specs=(
            P(SP, TP),
            P(),
            P(SP, TP),
            P(SP, TP),
            P(SP, TP),
            P(SP, TP),
            P(SP, TP),
            P(SP, TP),
            P(TP),
            P(SP, TP),
            P(TP),
            P(TP, None, None),
            P(TP),
            P(TP, SP),
            P(TP, SP),
            P(),
        ),
        out_specs=P(SP_TP, None),
        check_vma=False,
    )
```

profile of v0, /device:TPU:1, one launch (start us, length us, event | category | flops | bytes accessed | tf_op | source)
XLA Modules:
  0.0 284.9 jit_solution(16253742989583789362)
XLA Ops:
  6.5 1.3 pad_maximum_fusion.4
  7.9 0.7 constant_dynamic-update-slice_fusion.5
  8.6 0.7 constant_dynamic-update-slice_fusion.4
  9.3 0.7 constant_dynamic-update-slice_fusion.3
  10.0 0.7 constant_dynamic-update-slice_fusion.2
  10.8 0.7 constant_dynamic-update-slice_fusion.1
  11.5 0.7 constant_dynamic-update-slice_fusion
  12.2 0.6 copy-done.1
  12.9 0.9 fusion.167
  13.7 10.5 %all-gather = bf16[512,256]{1,0:T(8,128)(2,1)S(1)} all-gather(bf16[128,256]{1,0:T(8,128)(2,1)S(1)} %get-tuple-element.199), channel_id=2, replica_groups=mesh['sp_0'=8,'sp_1'=8,'tp_0'=4,'tp_1'=2] {'tp_0'}, dimensions={0}, use_global_device_ids=true | all-gather | bytes 327680 | tf_op jit(solution)/shard_map/all_gather | solution.py:33
  24.3 10.4 %all_gather.34 = bf16[8,128,256]{2,1,0:T(8,128)(2,1)S(1)} all-gather(bf16[4,128,256]{2,1,0:T(8,128)(2,1)S(1)} %bitcast.247), channel_id=1, replica_groups=mesh['sp_0'=8,'sp_1'=8,'tp_0'=4,'tp_1'=2] {'tp_1'}, dimensions={0}, use_global_device_ids=true | all-gather | bytes 786432 | tf_op jit(solution)/shard_map/all_gather | solution.py:33
  34.7 1.9 all-gather.1
  36.8 10.3 %all_gather.36 = bf16[8,128,256]{2,1,0:T(8,128)(2,1)S(1)} all-gather(bf16[2,128,256]{2,1,0:T(8,128)(2,1)S(1)} %bitcast.249), channel_id=1, replica_groups=mesh['sp_0'=8,'sp_1'=8,'tp_0'=4,'tp_1'=2] {'tp_0'}, dimensions={0}, use_global_device_ids=true | all-gather | bytes 655360 | tf_op jit(solution)/shard_map/all_gather | solution.py:33
  47.2 46.0 %all-gather.12.cloned.1.call-done = bf16[2048,256]{1,0:T(8,128)(2,1)} async-done(((bf16[32,256]{1,0:T(8,128)(2,1)}), bf16[2048,256]{1,0:T(8,128)(2,1)}) %all-gather.12.cloned.1.call-update) | async-done | bytes 1048592 | tf_op jit(solution)/shard_map/all_gather | solution.py:106
  93.2 1.3 slice_bitcast_fusion.2
  94.5 1.1 pad_maximum_fusion.1
  95.6 0.3 fusion.35
  96.0 1.9 copy.67
  98.1 1.9 fusion.36
  100.0 79.3 %all-gather.10.cloned.1.call-done = bf16[2048,768]{1,0:T(8,128)(2,1)} async-done(((bf16[32,768]{1,0:T(8,128)(2,1)}), bf16[2048,768]{1,0:T(8,128)(2,1)}) %all-gather.10.cloned.1.call-update) | async-done | bytes 3145744 | tf_op jit(solution)/shard_map/all_gather | solution.py:19
  179.3 2.9 %fusion.38 = bf16[256,768]{1,0:T(8,128)(2,1)S(1)} fusion(bf16[256,2048]{0,1:T(8,128)(2,1)S(1)} %fusion.36, bf16[2048,768]{1,0:T(8,128)(2,1)} %all-gather.10.cloned.1.call-done, f32[256]{0:T(256)S(1)} %add_rsqrt_fusion.1), kind=kOutput, calls=%fused_computation.54 | convolution fusion | flops 805699584 | bytes 4588544 | tf_op jit(solution)/shard_map/dot_general | solution.py:184
  182.3 2.7 collective-permute-start
  185.1 13.2 %while.17 = (s32[]{:T(128)}, f32[1,128,128]{2,1,0:T(8,128)S(1)}, f32[1,128]{1,0:T(1,128)S(1)}, f32[4,1,64,128]{3,2,1,0:T(8,128)S(1)}, f32[4,1,64,128]{3,2,1,0:T(...) while((s32[]{:T(128)}, f32[1,128,128]{2,1,0:T(8,128)S(1)}, ...), condition=%wide.region_3.4_spmd.clone, body=%wide.region_1.3_spmd.clone.sunk | while | flops 35234048 | bytes 5177500 | solution.py:153
  185.5 0.3 fusion.192
  185.8 0.6 exponential_select_fusion.2
  186.5 1.7 fusion.196
  188.2 0.2 fusion.197
  188.8 0.3 fusion.192
  189.1 0.6 exponential_select_fusion.2
  189.8 1.7 fusion.196
  191.5 0.2 fusion.197
  192.1 0.3 fusion.192
  192.4 0.6 exponential_select_fusion.2
  193.1 1.7 fusion.196
  194.8 0.2 fusion.197
  195.3 0.3 fusion.192
  195.7 0.6 exponential_select_fusion.2
  196.4 1.7 fusion.196
  198.1 0.2 fusion.197
  198.4 22.0 %all-gather.4 = f32[8,129,128]{2,1,0:T(8,128)S(1)} all-gather(f32[1,129,128]{2,1,0:T(8,128)S(1)} %maximum_bitcast_fusion), channel_id=4, replica_groups=mesh['sp_0'=8,'sp_1'=8,'tp_0'=4,'tp_1'=2] {'sp_1'}, dimensions={0}, use_global_device_ids=true | all-gather | bytes 594432 | tf_op jit(solution)/shard_map/all_gather | solution.py:72
  220.6 21.3 %all-gather.5 = f32[8,129,128]{2,1,0:T(8,128)S(1)} all-gather(f32[1,129,128]{2,1,0:T(8,128)S(1)} %maximum_bitcast_fusion.1), channel_id=5, replica_groups=mesh['sp_0'=8,'sp_1'=8,'tp_0'=4,'tp_1'=2] {'sp_0'}, dimensions={0}, use_global_device_ids=true | all-gather | bytes 594432 | tf_op jit(solution)/shard_map/all_gather | solution.py:72
  241.9 0.7 multiply_reduce_fusion.1
  242.9 0.4 fusion.41
  243.3 0.7 pad_maximum_fusion.3
  244.0 16.6 %all-to-all-start = ((bf16[8,32,256]{2,1,0:T(8,128)(2,1)}), bf16[8,32,256]{2,1,0:T(8,128)(2,1)S(1)}, u32[]{:S(2)}, u32[]{:S(2)}) async-start(bf16[8,32,256]{2,1,0:T(8,128)(2,1)} %bitcast.46), calls=%async_computation | async-start | bytes 262144 | tf_op jit(solution)/shard_map/all_to_all | solution.py:254
  260.6 11.9 %copy.74 = bf16[2048,2048]{1,0:T(8,128)(2,1)} copy(bf16[2048,2048]{0,1:T(8,128)(2,1)} %all-gather.14.cloned.1.call-done) | data formatting | bytes 16777216 | tf_op jit(solution)/shard_map/all_gather | solution.py:255
  272.5 4.9 %fusion.37 = f32[32,2048]{1,0:T(8,128)S(1)} fusion(bf16[8,256,2048]{2,1,0:T(8,128)(2,1)} %bitcast.239, bf16[8,32,256]{2,1,0:T(8,128)(2,1)S(1)} %all-to-all-done), kind=kOutput, calls=%fused_computation.52 | convolution fusion | flops 269942784 | bytes 8781824 | tf_op jit(solution)/shard_map/tjc,jcd->jtd/dot_general | solution.py:257
  277.6 0.8 multiply_convert_fusion
  (95 shorter events, 2.8 us)
Async XLA Ops:
  6.5 236.3 %copy-start = (bf16[1,128,128]{2,1,0:T(8,128)(2,1)S(1)}, bf16[1,128,128]{2,1,0:T(8,128)(2,1)}, u32[]{:S(2)}) copy-start(bf16[1,128,128]{2,1,0:T(8,128)(2,1)} %param.29) | copy-start | bytes 98308
  6.5 86.7 %all-gather.12.cloned.1.call-start = ((), (), s32[]{:S(2)}) async-start(), calls=%async_computation.2 | async-start | bytes 1064960 | tf_op jit(solution)/shard_map/all_gather | solution.py:106
  7.9 171.4 %all-gather.10.cloned.1.call-start = ((), (), s32[]{:S(2)}) async-start(), calls=%async_computation.1 | async-start | bytes 3194880 | tf_op jit(solution)/shard_map/all_gather | solution.py:19
  12.2 0.6 copy-start.1
  12.8 247.8 %all-gather.14.cloned.1.call-start = ((), (), s32[]{:S(2)}) async-start(), calls=%async_computation.3 | async-start | bytes 9437184 | tf_op jit(solution)/shard_map/all_gather | solution.py:255
  96.0 2.1 copy-start.6
  96.0 2.1 copy-start.2
  100.0 85.0 %copy-start.4 = (f32[256,1]{0,1:T(1,128)S(1)}, f32[256,1]{0,1:T(1,128)}, u32[]{:S(2)}) copy-start(f32[256,1]{0,1:T(1,128)} %param.27) | copy-start | bytes 3076
  182.3 60.6 %collective-permute-start = (bf16[16,128]{1,0:T(8,128)(2,1)S(1)}, bf16[16,128]{1,0:T(8,128)(2,1)S(1)}, u32[]{:S(2)}, u32[]{:S(2)}) collective-permute-start(bf16[16,128]{1,0:T(8,128)(2,1)S(1)} %slice.312), channel_id=1, source_target_pairs={{0,8},{8,16},{16,24},{24,32},{32,40},{40,48},{48,56},{56,64},{64,7... | collective-permute-start | bytes 12296 | tf_op jit(solution)/shard_map/ppermute | solution.py:99
  198.3 44.4 %copy-start.5 = (f32[128]{0:T(128)S(1)}, f32[128]{0:T(128)}, u32[]{:S(2)}) copy-start(f32[128]{0:T(128)} %param.28) | copy-start | bytes 1540
  198.3 44.5 %copy-start.7 = (f32[128]{0:T(128)S(1)}, f32[128]{0:T(128)}, u32[]{:S(2)}) copy-start(f32[128]{0:T(128)} %param.30) | copy-start | bytes 1540
  244.0 28.5 %all-to-all-start = ((bf16[8,32,256]{2,1,0:T(8,128)(2,1)}), bf16[8,32,256]{2,1,0:T(8,128)(2,1)S(1)}, u32[]{:S(2)}, u32[]{:S(2)}) async-start(bf16[8,32,256]{2,1,0:T(8,128)(2,1)} %bitcast.46), calls=%async_computation | async-start | bytes 262144 | tf_op jit(solution)/shard_map/all_to_all | solution.py:254
  272.5 5.1 %copy-start.3 = (f32[2048]{0:T(1024)S(1)}, f32[2048]{0:T(1024)}, u32[]{:S(2)}) copy-start(f32[2048]{0:T(1024)} %param.33) | copy-start | bytes 24580
Sparse Core Ops, SparseCore 0:
  10.4 82.7 all-gather.11
  96.2 83.0 all-gather.9
  181.5 59.5 all-gather.13
where the time goes:
time: 286 us; the launch traced here: 285 us
  waiting for transfers between devices  125 us (44%)
  blocking collectives  76.4 us (27%)
  local copies, waits for them, and re-layouts  21.1 us (7%)
  starting transfers between devices  19.4 us (7%)
  other arithmetic  16.9 us (6%)
  between operations  13.5 us (5%)
  matrix products  11.8 us (4%)
    all_gather x1, waiting for transfers between devices, in_one_piece(): out = lax.all_gather(both, axis, axis=dim, tiled=True)  79.3 us
    all_gather x1, waiting for transfers between devices, gather_turned(): out = lax.all_gather(both, axis, axis=0, tiled=True)  46 us
    all_gather x2, blocking collectives, all_in_one(): both, at, found = (lax.all_gather(jnp.concatenate(lines), axis), 0, {})  43.3 us
    all_gather x4, blocking collectives, all_blocks(): tiles = lax.all_gather(tiles, axes[k], axis=0, tiled=True)  33.1 us
    all_to_all x1, starting transfers between devices, per_device(): lax.all_to_all(both, TP, split_axis=0, concat_axis=1, tiled=True)  16.6 us
    all_gather x1, local copies, waits for them, and re-layouts, per_device(): whole = lax.all_gather(weight_cat, TP, axis=0, tiled=True)  11.9 us
    dot_general x4, other arithmetic, advance(): jnp.einsum('htk,hsk,htsk->hts', probe_segment, key_piece, weight, precisi...  6.81 us
  transfers between devices with their start and end apart: 5, of which 2 were waited for; matrix products, arithmetic and copies ran while one was open for 15% of the time, Pallas kernels for 0%

commit v1 on v0

--- a/solution.py
+++ b/solution.py
@@ -251,7 +251,9 @@
     both = jnp.concatenate([y_rec, y_pool], axis=1)
     weight_cat = jnp.concatenate(out_parts, axis=0)
     groups = lax.axis_size(TP)
-    exchanged = lax.all_to_all(both, TP, split_axis=0, concat_axis=1, tiled=True)
+    exchanged = jnp.concatenate(
+        lax.all_to_all(jnp.stack(jnp.split(both, lax.axis_size(TP), axis=0)), TP, 0, 0), axis=1
+    )
     whole = lax.all_gather(weight_cat, TP, axis=0, tiled=True)
     owned = exchanged.shape[0]
     terms = jnp.einsum(

time: 286 us -> 290 us (1.014)
  other arithmetic: 16.9 us -> 21.1 us
    unnamed x5 -> x12, other arithmetic: 0.03 us -> 4.29 us
  transfers between devices with their start and end apart: 5 -> 5, of which waited for: 2 -> 2; matrix products, arithmetic and copies ran while one was open for 15% -> 16% of each run, Pallas kernels for 0% -> 0%
where the time goes in v1:
time: 290 us; the launch traced here: 289 us
  waiting for transfers between devices  125 us (43%)
  blocking collectives  76.4 us (26%)
  local copies, waits for them, and re-layouts  21.1 us (7%)
  other arithmetic  21.1 us (7%)
  starting transfers between devices  19.4 us (7%)
  between operations  13.5 us (5%)
  matrix products  11.8 us (4%)
    all_gather x1, waiting for transfers between devices, in_one_piece(): out = lax.all_gather(both, axis, axis=dim, tiled=True)  79.7 us
    all_gather x1, waiting for transfers between devices, gather_turned(): out = lax.all_gather(both, axis, axis=0, tiled=True)  45.6 us
    all_gather x2, blocking collectives, all_in_one(): both, at, found = (lax.all_gather(jnp.concatenate(lines), axis), 0, {})  43.3 us
    all_gather x4, blocking collectives, all_blocks(): tiles = lax.all_gather(tiles, axes[k], axis=0, tiled=True)  33.1 us
    all_to_all x1, starting transfers between devices, per_device(): lax.all_to_all(jnp.stack(jnp.split(both, lax.axis_size(TP), axis=0)), TP,...  16.6 us
    all_gather x1, local copies, waits for them, and re-layouts, per_device(): whole = lax.all_gather(weight_cat, TP, axis=0, tiled=True)  11.9 us
    dot_general x4, other arithmetic, advance(): jnp.einsum('htk,hsk,htsk->hts', probe_segment, key_piece, weight, precisi...  6.81 us
  transfers between devices with their start and end apart: 5, of which 2 were waited for; matrix products, arithmetic and copies ran while one was open for 16% of the time, Pallas kernels for 0%

profile of v1, /device:TPU:1, one launch (start us, length us, event | category | flops | bytes accessed | tf_op | source)
XLA Modules:
  0.0 289.1 jit_solution(1886598099277732226)
XLA Ops:
  6.5 1.3 pad_maximum_fusion.4
  7.9 0.7 constant_dynamic-update-slice_fusion.5
  8.6 0.7 constant_dynamic-update-slice_fusion.4
  9.3 0.7 constant_dynamic-update-slice_fusion.3
  10.0 0.7 constant_dynamic-update-slice_fusion.2
  10.8 0.7 constant_dynamic-update-slice_fusion.1
  11.5 0.7 constant_dynamic-update-slice_fusion
  12.2 0.6 copy-done.1
  12.9 0.9 fusion.175
  13.7 10.5 %all-gather = bf16[512,256]{1,0:T(8,128)(2,1)S(1)} all-gather(bf16[128,256]{1,0:T(8,128)(2,1)S(1)} %get-tuple-element.199), channel_id=2, replica_groups=mesh['sp_0'=8,'sp_1'=8,'tp_0'=4,'tp_1'=2] {'tp_0'}, dimensions={0}, use_global_device_ids=true | all-gather | bytes 327680 | tf_op jit(solution)/shard_map/all_gather | solution.py:33
  24.3 10.4 %all_gather.34 = bf16[8,128,256]{2,1,0:T(8,128)(2,1)S(1)} all-gather(bf16[4,128,256]{2,1,0:T(8,128)(2,1)S(1)} %bitcast.264), channel_id=1, replica_groups=mesh['sp_0'=8,'sp_1'=8,'tp_0'=4,'tp_1'=2] {'tp_1'}, dimensions={0}, use_global_device_ids=true | all-gather | bytes 786432 | tf_op jit(solution)/shard_map/all_gather | solution.py:33
  34.7 1.9 all-gather.1
  36.6 10.3 %all_gather.36 = bf16[8,128,256]{2,1,0:T(8,128)(2,1)S(1)} all-gather(bf16[2,128,256]{2,1,0:T(8,128)(2,1)S(1)} %bitcast.266), channel_id=1, replica_groups=mesh['sp_0'=8,'sp_1'=8,'tp_0'=4,'tp_1'=2] {'tp_0'}, dimensions={0}, use_global_device_ids=true | all-gather | bytes 655360 | tf_op jit(solution)/shard_map/all_gather | solution.py:33
  47.6 45.6 %all-gather.12.cloned.1.call-done = bf16[2048,256]{1,0:T(8,128)(2,1)} async-done(((bf16[32,256]{1,0:T(8,128)(2,1)}), bf16[2048,256]{1,0:T(8,128)(2,1)}) %all-gather.12.cloned.1.call-update) | async-done | bytes 1048592 | tf_op jit(solution)/shard_map/all_gather | solution.py:106
  93.2 1.3 slice_bitcast_fusion.2
  94.5 1.1 pad_maximum_fusion.1
  95.7 1.9 copy.67
  97.7 1.9 fusion.36
  99.6 79.7 %all-gather.10.cloned.1.call-done = bf16[2048,768]{1,0:T(8,128)(2,1)} async-done(((bf16[32,768]{1,0:T(8,128)(2,1)}), bf16[2048,768]{1,0:T(8,128)(2,1)}) %all-gather.10.cloned.1.call-update) | async-done | bytes 3145744 | tf_op jit(solution)/shard_map/all_gather | solution.py:19
  179.3 2.9 %fusion.38 = bf16[256,768]{1,0:T(8,128)(2,1)S(1)} fusion(bf16[256,2048]{0,1:T(8,128)(2,1)S(1)} %fusion.36, bf16[2048,768]{1,0:T(8,128)(2,1)} %all-gather.10.cloned.1.call-done, f32[256]{0:T(256)S(1)} %add_rsqrt_fusion.1), kind=kOutput, calls=%fused_computation.54 | convolution fusion | flops 805699584 | bytes 4588544 | tf_op jit(solution)/shard_map/dot_general | solution.py:184
  182.3 2.7 collective-permute-start
  185.1 13.2 %while.17 = (s32[]{:T(128)}, f32[1,128,128]{2,1,0:T(8,128)S(1)}, f32[1,128]{1,0:T(1,128)S(1)}, f32[4,1,64,128]{3,2,1,0:T(8,128)S(1)}, f32[4,1,64,128]{3,2,1,0:T(...) while((s32[]{:T(128)}, f32[1,128,128]{2,1,0:T(8,128)S(1)}, ...), condition=%wide.region_3.4_spmd.clone, body=%wide.region_1.3_spmd.clone.sunk | while | flops 35234048 | bytes 5177500 | solution.py:153
  185.8 0.6 exponential_select_fusion.2
  186.5 1.7 fusion.204
  188.8 0.3 fusion.200
  189.1 0.6 exponential_select_fusion.2
  189.8 1.7 fusion.204
  192.4 0.6 exponential_select_fusion.2
  193.1 1.7 fusion.204
  195.3 0.3 fusion.200
  195.7 0.6 exponential_select_fusion.2
  196.4 1.7 fusion.204
  198.4 22.0 %all-gather.4 = f32[8,129,128]{2,1,0:T(8,128)S(1)} all-gather(f32[1,129,128]{2,1,0:T(8,128)S(1)} %maximum_bitcast_fusion), channel_id=4, replica_groups=mesh['sp_0'=8,'sp_1'=8,'tp_0'=4,'tp_1'=2] {'sp_1'}, dimensions={0}, use_global_device_ids=true | all-gather | bytes 594432 | tf_op jit(solution)/shard_map/all_gather | solution.py:72
  220.6 21.3 %all-gather.5 = f32[8,129,128]{2,1,0:T(8,128)S(1)} all-gather(f32[1,129,128]{2,1,0:T(8,128)S(1)} %maximum_bitcast_fusion.1), channel_id=5, replica_groups=mesh['sp_0'=8,'sp_1'=8,'tp_0'=4,'tp_1'=2] {'sp_0'}, dimensions={0}, use_global_device_ids=true | all-gather | bytes 594432 | tf_op jit(solution)/shard_map/all_gather | solution.py:72
  241.9 0.7 multiply_reduce_fusion.1
  242.9 0.4 fusion.41
  243.3 0.6 constant_dynamic-update-slice_fusion.13
  243.9 0.6 constant_dynamic-update-slice_fusion.12
  244.5 0.6 constant_dynamic-update-slice_fusion.11
  245.1 0.6 constant_dynamic-update-slice_fusion.10
  245.7 0.6 constant_dynamic-update-slice_fusion.9
  246.4 0.6 constant_dynamic-update-slice_fusion.8
  247.0 0.6 constant_dynamic-update-slice_fusion.7
  247.6 0.6 constant_dynamic-update-slice_fusion.6
  248.2 16.6 %all-to-all-start = ((bf16[8,32,256]{2,1,0:T(8,128)(2,1)}), bf16[8,32,256]{2,1,0:T(8,128)(2,1)S(1)}, u32[]{:S(2)}, u32[]{:S(2)}) async-start(bf16[8,32,256]{2,1,0:T(8,128)(2,1)} %constant_dynamic-update-slice_fusion.6), calls=%async_computation | async-start | bytes 262144 | tf_op jit(solution)/shard_map/all_to_all | solution.py:255
  264.8 11.9 %copy.74 = bf16[2048,2048]{1,0:T(8,128)(2,1)} copy(bf16[2048,2048]{0,1:T(8,128)(2,1)} %all-gather.14.cloned.1.call-done) | data formatting | bytes 16777216 | tf_op jit(solution)/shard_map/all_gather | solution.py:257
  276.7 4.9 %fusion.37 = f32[32,2048]{1,0:T(8,128)S(1)} fusion(bf16[8,256,2048]{2,1,0:T(8,128)(2,1)} %bitcast.256, bf16[8,32,256]{2,1,0:T(8,128)(2,1)S(1)} %all-to-all-done), kind=kOutput, calls=%fused_computation.52 | convolution fusion | flops 269942784 | bytes 8781824 | tf_op jit(solution)/shard_map/tjc,jcd->jtd/dot_general | solution.py:259
  281.8 0.8 multiply_convert_fusion
  (102 shorter events, 4.6 us)
Async XLA Ops:
  6.5 236.3 %copy-start = (bf16[1,128,128]{2,1,0:T(8,128)(2,1)S(1)}, bf16[1,128,128]{2,1,0:T(8,128)(2,1)}, u32[]{:S(2)}) copy-start(bf16[1,128,128]{2,1,0:T(8,128)(2,1)} %param.29) | copy-start | bytes 98308
  6.5 86.7 %all-gather.12.cloned.1.call-start = ((), (), s32[]{:S(2)}) async-start(), calls=%async_computation.2 | async-start | bytes 1064960 | tf_op jit(solution)/shard_map/all_gather | solution.py:106
  7.9 171.4 %all-gather.10.cloned.1.call-start = ((), (), s32[]{:S(2)}) async-start(), calls=%async_computation.1 | async-start | bytes 3194880 | tf_op jit(solution)/shard_map/all_gather | solution.py:19
  12.2 0.6 copy-start.1
  12.8 252.0 %all-gather.14.cloned.1.call-start = ((), (), s32[]{:S(2)}) async-start(), calls=%async_computation.3 | async-start | bytes 9437184 | tf_op jit(solution)/shard_map/all_gather | solution.py:257
  46.9 0.7 copy-start.6
  95.7 2.0 copy-start.2
  99.6 85.4 %copy-start.4 = (f32[256,1]{0,1:T(1,128)S(1)}, f32[256,1]{0,1:T(1,128)}, u32[]{:S(2)}) copy-start(f32[256,1]{0,1:T(1,128)} %param.27) | copy-start | bytes 3076
  182.3 60.6 %collective-permute-start = (bf16[16,128]{1,0:T(8,128)(2,1)S(1)}, bf16[16,128]{1,0:T(8,128)(2,1)S(1)}, u32[]{:S(2)}, u32[]{:S(2)}) collective-permute-start(bf16[16,128]{1,0:T(8,128)(2,1)S(1)} %slice.312), channel_id=1, source_target_pairs={{0,8},{8,16},{16,24},{24,32},{32,40},{40,48},{48,56},{56,64},{64,7... | collective-permute-start | bytes 12296 | tf_op jit(solution)/shard_map/ppermute | solution.py:99
  198.3 44.4 %copy-start.5 = (f32[128]{0:T(128)S(1)}, f32[128]{0:T(128)}, u32[]{:S(2)}) copy-start(f32[128]{0:T(128)} %param.28) | copy-start | bytes 1540
  198.3 44.5 %copy-start.7 = (f32[128]{0:T(128)S(1)}, f32[128]{0:T(128)}, u32[]{:S(2)}) copy-start(f32[128]{0:T(128)} %param.30) | copy-start | bytes 1540
  248.2 28.5 %all-to-all-start = ((bf16[8,32,256]{2,1,0:T(8,128)(2,1)}), bf16[8,32,256]{2,1,0:T(8,128)(2,1)S(1)}, u32[]{:S(2)}, u32[]{:S(2)}) async-start(bf16[8,32,256]{2,1,0:T(8,128)(2,1)} %constant_dynamic-update-slice_fusion.6), calls=%async_computation | async-start | bytes 262144 | tf_op jit(solution)/shard_map/all_to_all | solution.py:255
  276.7 5.1 %copy-start.3 = (f32[2048]{0:T(1024)S(1)}, f32[2048]{0:T(1024)}, u32[]{:S(2)}) copy-start(f32[2048]{0:T(1024)} %param.33) | copy-start | bytes 24580
Sparse Core Ops, SparseCore 0:
  10.4 82.7 all-gather.11
  96.2 83.0 all-gather.9
  181.5 59.5 all-gather.13
